TPU v7x, 32 devices: a whole 2x2x4 slice. The times are simulated.
32 devices in a mesh: ep: 4 (over y, x), tp: 8 (over z, core).
Axes of the slice: x: 2, y: 2, z: 4, core: 2. Of those that a mesh axis runs over, the one named last changes fastest.
Arguments:
- tokens: bfloat16 [256, 4096], P('ep'), may hold values from -6 to 6
- norm_gain: float32 [4096], replicated, may hold values from 0.1 to 1.9
- ffn_gain: float32 [4096], replicated, may hold values from 0.1 to 1.9
- w_in: bfloat16 [4096, 2048], P(None, 'tp'), may hold values from -0.09375 to 0.09375
- decay_rate: float32 [8192], P('tp'), may hold values from 0.02 to 2
- frequency: float32 [8192], P('tp'), may hold values from -3.140625 to 3.140625
- log_step: float32 [128], P('tp'), may hold values from -2.3 to 0
- input_real: float32 [16, 8192], P(None, 'tp'), may hold values from -1 to 1
- input_imag: float32 [16, 8192], P(None, 'tp'), may hold values from -1 to 1
- readout_real: float32 [16, 8192], P(None, 'tp'), may hold values from -0.5 to 0.5
- readout_imag: float32 [16, 8192], P(None, 'tp'), may hold values from -0.5 to 0.5
- skip_gain: float32 [2048], P('tp'), may hold values from -4 to 4
- state_real: float32 [256, 8192], P('ep', 'tp'), may hold values from -6 to 6
- state_imag: float32 [256, 8192], P('ep', 'tp'), may hold values from -6 to 6
- w_out: bfloat16 [2048, 4096], P('tp'), may hold values from -0.125 to 0.125
- shared_gate: bfloat16 [4096, 1024], P(None, 'tp'), may hold values from -0.09375 to 0.09375
- shared_up: bfloat16 [4096, 1024], P(None, 'tp'), may hold values from -0.09375 to 0.09375
- shared_down: bfloat16 [1024, 4096], P('tp'), may hold values from -0.1875 to 0.1875
- expert_gate: bfloat16 [16, 4096, 1024], P('ep', 'tp'), may hold values from -0.09375 to 0.09375
- expert_up: bfloat16 [16, 4096, 1024], P('ep', 'tp'), may hold values from -0.09375 to 0.09375
- expert_down: bfloat16 [16, 1024, 4096], P('ep', None, 'tp'), may hold values from -0.1875 to 0.1875
- routing: int32 [256, 4], P('ep'), may hold values from 0 to 15, all different within a row; in each aligned block of 64 rows (0 to 63, 64 to 127, ...) at most 32 rows name the same one
- route_weight: float32 [256, 4], P('ep'), may hold values from 0.1 to 1
Outputs:
- mixed: bfloat16 [256, 4096], P('ep', 'tp')
- new_state_real: float32 [256, 8192], P('ep', 'tp')
- new_state_imag: float32 [256, 8192], P('ep', 'tp')
Inputs may be any that keep to these rules, and one draw needn't show every extreme that they name: `routing`: each row names 4 different experts. In the rows of one index of ep (aligned blocks of 64 rows) no expert is named more than 32 times, and in every draw some expert is named exactly 32 times in some block.
All inputs are finite; a program needn't handle non-finite values.
Results may differ from a plain program's by a relative error of at most 0.02.
Values may be sent and summed in bfloat16 or wider, within the bound.
A program may use at most 64 MiB of HBM per device.

v0:
```python
import jax
import jax.numpy as jnp
from jax import lax
from jax.sharding import PartitionSpec as P

EPS = 1e-06
ROUTED_SCALE = 2.5
HIGH = lax.Precision.HIGHEST


def rms_scale(values_in, gains):
    values = values_in.astype(jnp.float32)
    factor = lax.rsqrt(jnp.mean(values * values, axis=-1, keepdims=True) + EPS)
    return (values * factor * gains).astype(jnp.bfloat16)


def state_update(
    normed,
    w_in,
    decay_rate,
    frequency,
    log_step,
    input_real,
    input_imag,
    readout_real,
    readout_imag,
    skip_gain,
    state_real,
    state_imag,
):
    seq_count = normed.shape[0]
    groups = log_step.shape[0]
    chan_count = skip_gain.shape[0] // groups
    state_width = decay_rate.shape[0] // groups
    drive_rows = jnp.dot(normed, w_in, preferred_element_type=jnp.float32).astype(jnp.bfloat16)
    drive_f = drive_rows.astype(jnp.float32).reshape(seq_count, groups, chan_count)
    decays = decay_rate.reshape(groups, state_width)
    omegas = frequency.reshape(groups, state_width)
    step_size = jnp.exp(log_step)[:, None]
    pole_mag = jnp.exp(-decays * step_size)
    pole_angle = omegas * step_size
    pole_re = pole_mag * jnp.cos(pole_angle)
    pole_im = pole_mag * jnp.sin(pole_angle)
    pole_norm = decays * decays + omegas * omegas
    diff_re = pole_re - 1.0
    lift_re = (-decays * diff_re + omegas * pole_im) / pole_norm
    lift_im = (-decays * pole_im - omegas * diff_re) / pole_norm
    in_re = input_real.reshape(chan_count, groups, state_width)
    in_im = input_imag.reshape(chan_count, groups, state_width)
    push_re = jnp.einsum("sgh,hgp->sgp", drive_f, in_re, precision=HIGH)
    push_im = jnp.einsum("sgh,hgp->sgp", drive_f, in_im, precision=HIGH)
    old_re = state_real.reshape(seq_count, groups, state_width)
    old_im = state_imag.reshape(seq_count, groups, state_width)
    new_re = pole_re * old_re - pole_im * old_im + lift_re * push_re - lift_im * push_im
    new_im = pole_re * old_im + pole_im * old_re + lift_re * push_im + lift_im * push_re
    out_re = readout_real.reshape(chan_count, groups, state_width)
    out_im = readout_imag.reshape(chan_count, groups, state_width)
    read_rows = jnp.einsum("sgp,hgp->sgh", new_re, out_re, precision=HIGH) - jnp.einsum(
        "sgp,hgp->sgh", new_im, out_im, precision=HIGH
    )
    read_rows = read_rows + skip_gain.reshape(groups, chan_count) * drive_f
    activated = jax.nn.gelu(read_rows).reshape(seq_count, groups * chan_count).astype(jnp.bfloat16)
    return (
        activated,
        new_re.reshape(seq_count, groups * state_width),
        new_im.reshape(seq_count, groups * state_width),
    )


def local(
    tokens,
    norm_gain,
    ffn_gain,
    w_in,
    decay_rate,
    frequency,
    log_step,
    input_real,
    input_imag,
    readout_real,
    readout_imag,
    skip_gain,
    state_real,
    state_imag,
    w_out,
    shared_gate,
    shared_up,
    shared_down,
    expert_gate,
    expert_up,
    expert_down,
    routing,
    route_weight,
):
    seq_count, model_width = tokens.shape
    tp_count = lax.axis_size("tp")
    ep_count = lax.axis_size("ep")
    slice_width = model_width // tp_count
    offset = lax.axis_index("tp") * slice_width
    normed = rms_scale(tokens, norm_gain)
    activated, new_real, new_imag = state_update(
        normed,
        w_in,
        decay_rate,
        frequency,
        log_step,
        input_real,
        input_imag,
        readout_real,
        readout_imag,
        skip_gain,
        state_real,
        state_imag,
    )
    mixer_terms = jnp.dot(activated, w_out, preferred_element_type=jnp.float32)
    mixer_own = lax.psum_scatter(mixer_terms, "tp", scatter_dimension=1, tiled=True)
    own_tokens = lax.dynamic_slice_in_dim(tokens, offset, slice_width, 1)
    resid_own = (own_tokens.astype(jnp.float32) + mixer_own).astype(jnp.bfloat16)
    resid_f = resid_own.astype(jnp.float32)
    square_sum = lax.psum(jnp.sum(resid_f * resid_f, axis=1, keepdims=True), "tp")
    factor = lax.rsqrt(square_sum / model_width + EPS)
    gain_own = lax.dynamic_slice_in_dim(ffn_gain, offset, slice_width, 0)
    rows_own = (resid_f * factor * gain_own).astype(jnp.bfloat16)
    ffn_rows = lax.all_gather(rows_own, "tp", axis=1, tiled=True)
    expert_dev = expert_gate.shape[0]
    expert_count = expert_dev * ep_count
    top_count = routing.shape[1]
    capacity = 2 * seq_count * top_count // expert_count
    slot_count = expert_count * capacity
    flat_ids = routing.reshape(-1)
    one_hot = (flat_ids[:, None] == jnp.arange(expert_count, dtype=jnp.int32)[None, :]).astype(
        jnp.int32
    )
    earlier = jnp.cumsum(one_hot, axis=0) - one_hot
    slot_rank = jnp.sum(earlier * one_hot, axis=1)
    target = flat_ids * capacity + slot_rank
    slot_ids = jnp.arange(slot_count, dtype=jnp.int32)
    placed = (target[None, :] == slot_ids[:, None]).reshape(slot_count, seq_count, top_count)
    dispatch_map = jnp.sum(placed.astype(jnp.float32), axis=2).astype(jnp.bfloat16)
    outgoing = jnp.dot(dispatch_map, rows_own, preferred_element_type=jnp.float32).astype(
        jnp.bfloat16
    )
    outgoing = outgoing.reshape(ep_count, expert_dev * capacity, slice_width)
    incoming = lax.all_to_all(outgoing, "ep", split_axis=0, concat_axis=0, tiled=True)
    arrived = incoming.reshape(ep_count, expert_dev, capacity, slice_width)
    gate_part = jnp.einsum(
        "secd,edf->secf", arrived, expert_gate, preferred_element_type=jnp.float32
    )
    up_part = jnp.einsum("secd,edf->secf", arrived, expert_up, preferred_element_type=jnp.float32)
    gate_full, up_full = (
        lax.psum(gate_part.astype(jnp.bfloat16), "tp").astype(jnp.float32),
        lax.psum(up_part.astype(jnp.bfloat16), "tp").astype(jnp.float32),
    )
    inner_rows = (jax.nn.silu(gate_full) * up_full).astype(jnp.bfloat16)
    expert_terms = jnp.einsum(
        "secf,efd->secd", inner_rows, expert_down, preferred_element_type=jnp.float32
    )
    returned = lax.all_to_all(
        expert_terms.reshape(ep_count, expert_dev * capacity, slice_width).astype(jnp.bfloat16),
        "ep",
        split_axis=0,
        concat_axis=0,
        tiled=True,
    ).astype(jnp.float32)
    weights = route_weight / jnp.sum(route_weight, axis=1, keepdims=True) * ROUTED_SCALE
    chosen = target.reshape(seq_count, top_count)[:, :, None] == slot_ids[None, None, :]
    combine = jnp.sum(jnp.where(chosen, weights[:, :, None], 0.0), axis=1)
    routed = jnp.dot(combine, returned.reshape(slot_count, slice_width), precision=HIGH)
    shared_gate_rows = jnp.dot(ffn_rows, shared_gate, preferred_element_type=jnp.float32)
    shared_up_rows = jnp.dot(ffn_rows, shared_up, preferred_element_type=jnp.float32)
    shared_inner = (jax.nn.silu(shared_gate_rows) * shared_up_rows).astype(jnp.bfloat16)
    shared_terms = jnp.dot(shared_inner, shared_down, preferred_element_type=jnp.float32)
    shared_own = lax.psum_scatter(
        shared_terms.astype(jnp.bfloat16), "tp", scatter_dimension=1, tiled=True
    ).astype(jnp.float32)
    mixed = (resid_own.astype(jnp.float32) + shared_own + routed).astype(jnp.bfloat16)
    return (mixed, new_real, new_imag)


def solution(mesh):
    placed = (
        P("ep", None),
        P(),
        P(),
        P(None, "tp"),
        P("tp"),
        P("tp"),
        P("tp"),
        P(None, "tp"),
        P(None, "tp"),
        P(None, "tp"),
        P(None, "tp"),
        P("tp"),
        P("ep", "tp"),
        P("ep", "tp"),
        P("tp", None),
        P(None, "tp"),
        P(None, "tp"),
        P("tp", None),
        P("ep", "tp", None),
        P("ep", "tp", None),
        P("ep", None, "tp"),
        P("ep", None),
        P("ep", None),
    )
    return jax.shard_map(
        local,
        mesh=mesh,
        in_specs=placed,
        out_specs=(P("ep", "tp"), P("ep", "tp"), P("ep", "tp")),
        check_vma=False,
    )
```

profile of v0, /device:TPU:0, one launch (start us, length us, event | category | flops | bytes accessed | tf_op | source)
XLA Modules:
  0.0 197.0 jit_solution(18267901409263895610)
XLA Ops:
  7.3 0.8 exp.27
  8.1 1.2 fusion.34
  9.4 0.8 reshape.245
  10.1 0.8 mul.328
  10.9 0.7 fusion.74
  11.7 2.3 %convolution_convert_fusion.2 = bf16[64,256]{1,0:T(8,128)(2,1)S(1)} fusion(bf16[4096,256]{1,0:T(8,128)(2,1)} %param.26, bf16[64,4096]{1,0:T(8,128)(2,1)} %param.23, f32[4096]{0:T(1024)} %param.24, f32[64]{0:T(128)S(1)} %add_rsqrt_fusion), kind=kOutput, calls=%fused_computation.28 | convolution fusion | flops 135282688 | bytes 2670848 | tf_op jit(solution)/shard_map/dot_general | solution.py:35
  14.4 0.7 reshape.251
  15.2 1.0 reshape.246
  16.1 0.9 reshape.247
  17.6 1.9 bitcast_add_fusion
  19.6 0.9 fusion.55
  20.5 1.0 fusion.50
  21.5 1.5 fusion.75
  24.6 0.8 dynamic_slice.7
  25.5 33.1 %reduce-scatter.3.cloned.1.call-done = f32[64,512]{1,0:T(8,128)} async-done(((f32[64,4096]{1,0:T(8,128)}), f32[64,512]{1,0:T(8,128)}) %reduce-scatter.3.cloned.1.call-update) | async-done | bytes 131088 | tf_op jit(solution)/shard_map/reduce_scatter | solution.py:116
  58.5 1.0 fusion.51
  59.6 13.9 %psum.21 = f32[64,1]{0,1:T(1,128)S(1)} all-reduce(f32[64,1]{0,1:T(1,128)S(1)} %bitcast.105), channel_id=1, replica_groups=mesh['ep'=4,'tp'=8] {'tp'}, use_global_device_ids=true, to_apply=%region_3.0 | all-reduce | flops 64 | bytes 512 | tf_op jit(solution)/shard_map/psum | solution.py:120
  73.9 11.7 %all_to_all.10 = bf16[4,128,512]{2,1,0:T(8,128)(2,1)S(1)} all-to-all(bf16[4,128,512]{2,1,0:T(8,128)(2,1)S(1)} %bitcast.99), channel_id=1, replica_groups=mesh['ep'=4,'tp'=8] {'ep'}, dimensions={0} | all-to-all | bytes 1048576 | tf_op jit(solution)/shard_map/all_to_all | solution.py:144
  85.6 4.0 %fusion.17 = bf16[4,4,32,1024]{3,2,0,1:T(8,128)(2,1)} fusion(bf16[4,512,1024]{2,1,0:T(8,128)(2,1)} %param.42, bf16[4,4,32,512]{3,2,1,0:T(8,128)(2,1)S(1)} %bitcast.97), kind=kOutput, calls=%fused_computation.16 | convolution fusion | flops 537395200 | bytes 5767168 | tf_op jit(solution)/shard_map/secd,edf->secf/dot_general | solution.py:149
  89.6 1.7 fusion.20
  91.4 16.5 %all_gather.3 = bf16[64,4096]{1,0:T(8,128)(2,1)S(1)} all-gather(bf16[64,512]{1,0:T(8,128)(2,1)S(1)} %fusion.53), channel_id=1, replica_groups=mesh['ep'=4,'tp'=8] {'tp'}, dimensions={1}, use_global_device_ids=true | all-gather | bytes 589824 | tf_op jit(solution)/shard_map/all_gather | solution.py:124
  107.9 1.5 fusion.76
  109.5 3.0 %convolution_convert_fusion = bf16[64,4096]{1,0:T(8,128)(2,1)} fusion(bf16[128,4096]{1,0:T(8,128)(2,1)} %param.40, bf16[64,4096]{1,0:T(8,128)(2,1)S(1)} %all_gather.3, bf16[4096,128]{1,0:T(8,128)(2,1)} %param.39, f32[64,128]{1,0:T(8,128)S(1)} %fusion.76), kind=kOutput, calls=%fused_computation | convolution fusion | flops 134529024 | bytes 3178496 | tf_op jit(solution)/shard_map/dot_general | solution.py:172
  112.5 42.7 %all-reduce.3.cloned.1.call-done = (bf16[4,4,32,1024]{3,2,0,1:T(8,128)(2,1)}, bf16[4,4,32,1024]{3,2,0,1:T(8,128)(2,1)}) async-done(((bf16[4,4,32,1024]{3,2,0,1:T(8,128)(2,1)}, bf16[4,4,32,1024]{3,2,0,1:T(8,128)(2,1)}), (bf16[4,4,32,1024]{3,2,0,1:T(8,128)(2,1)}, bf16[4,4,32,1024]{3,2,0,1:T(8,128)(2,1)})) %all-reduce.3.cloned.1.call-update) | async-done | bytes 2097168 | tf_op jit(solution)/shard_map/psum | solution.py:152
  155.1 3.7 %fusion.26 = bf16[4,4,32,512]{3,2,0,1:T(8,128)(2,1)S(1)} fusion(bf16[4,1024,512]{2,1,0:T(8,128)(2,1)} %param.43, bf16[4,4,32,1024]{3,2,0,1:T(8,128)(2,1)} %get-tuple-element.3, bf16[4,4,32,1024]{3,2,0,1:T(8,128)(2,1)} %get-tuple-element.4), kind=kOutput, calls=%fused_computation.22 | convolution fusion | flops 541327360 | bytes 6815744 | tf_op jit(solution)/shard_map/secf,efd->secd/dot_general | solution.py:155
  158.9 0.9 copy.91
  159.7 4.1 %all-to-all-start.1 = ((bf16[4,128,512]{2,1,0:T(8,128)(2,1)}), bf16[4,128,512]{2,1,0:T(8,128)(2,1)}, u32[]{:S(2)}, u32[]{:S(2)}) async-start(bf16[4,128,512]{2,1,0:T(8,128)(2,1)} %bitcast.100), calls=%async_computation.3 | async-start | bytes 1048576 | tf_op jit(solution)/shard_map/all_to_all | solution.py:158
  163.9 1.1 copy.93
  165.3 1.9 reshape.259
  167.2 0.9 reshape.258
  168.3 20.2 %reduce-scatter.5.cloned.1.call-done = bf16[64,512]{1,0:T(8,128)(2,1)} async-done(((bf16[64,4096]{1,0:T(8,128)(2,1)}), bf16[64,512]{1,0:T(8,128)(2,1)}) %reduce-scatter.5.cloned.1.call-update) | async-done | bytes 65552 | tf_op jit(solution)/shard_map/reduce_scatter | solution.py:173
  188.4 2.1 %fusion.31 = bf16[64,512]{1,0:T(8,128)(2,1)} fusion(f32[64,512]{1,0:T(8,128)S(1)} %select_reduce_fusion, bf16[512,512]{1,0:T(8,128)(2,1)} %bitcast.22, bf16[64,512]{1,0:T(8,128)(2,1)S(1)} %get-tuple-element.6, bf16[64,512]{1,0:T(8,128)(2,1)} %reduce-scatter.5.cloned.1.call-done), kind=kOutput, calls=%fused_computation.27 | convolution fusion | flops 201490432 | bytes 851968 | tf_op jit(solution)/shard_map/dot_general | solution.py:168
  (62 shorter events, 3.7 us)
Async XLA Ops:
  7.2 14.4 %copy-start = (bf16[256,4096]{1,0:T(8,128)(2,1)S(1)}, bf16[256,4096]{1,0:T(8,128)(2,1)}, u32[]{:S(2)}) copy-start(bf16[256,4096]{1,0:T(8,128)(2,1)} %param.37) | copy-start | bytes 6291460
  7.2 7.0 %copy-start.7 = (f32[16,1024]{1,0:T(8,128)S(1)}, f32[16,1024]{1,0:T(8,128)}, u32[]{:S(2)}) copy-start(f32[16,1024]{1,0:T(8,128)} %param.30) | copy-start | bytes 196612
  7.2 7.1 %copy-start.8 = (f32[16,1024]{1,0:T(8,128)S(1)}, f32[16,1024]{1,0:T(8,128)}, u32[]{:S(2)}) copy-start(f32[16,1024]{1,0:T(8,128)} %param.31) | copy-start | bytes 196612
  7.2 7.2 %copy-start.9 = (f32[16,1024]{1,0:T(8,128)S(1)}, f32[16,1024]{1,0:T(8,128)}, u32[]{:S(2)}) copy-start(f32[16,1024]{1,0:T(8,128)} %param.32) | copy-start | bytes 196612
  7.2 7.9 %copy-start.10 = (f32[16,1024]{1,0:T(8,128)S(1)}, f32[16,1024]{1,0:T(8,128)}, u32[]{:S(2)}) copy-start(f32[16,1024]{1,0:T(8,128)} %param.33) | copy-start | bytes 196612
  7.2 8.0 %copy-start.5 = (f32[64,1024]{1,0:T(8,128)S(1)}, f32[64,1024]{1,0:T(8,128)}, u32[]{:S(2)}) copy-start(f32[64,1024]{1,0:T(8,128)} %param.35) | copy-start | bytes 786436
  7.2 51.3 %reduce-scatter.3.cloned.1.call-start = ((), (), s32[]{:S(2)}) async-start(), calls=%async_computation.4 | async-start | bytes 1179648 | tf_op jit(solution)/shard_map/reduce_scatter | solution.py:116
  11.7 4.4 %copy-start.6 = (f32[64,1024]{1,0:T(8,128)S(1)}, f32[64,1024]{1,0:T(8,128)}, u32[]{:S(2)}) copy-start(f32[64,1024]{1,0:T(8,128)} %param.36) | copy-start | bytes 786436
  17.1 2.5 %copy-start.4 = (f32[16,16,64]{2,1,0:T(8,128)S(1)}, f32[16,16,64]{2,1,0:T(8,128)}, u32[]{:S(2)}) copy-start(f32[16,16,64]{2,1,0:T(8,128)} %reshape.251) | copy-start | bytes 196612
  19.6 3.5 %copy-start.1 = (f32[64,16,64]{2,0,1:T(8,128)}, f32[64,16,64]{2,0,1:T(8,128)S(1)}, u32[]{:S(2)}) copy-start(f32[64,16,64]{2,0,1:T(8,128)S(1)} %get-tuple-element.7) | copy-start | bytes 786436
  21.5 1.6 copy-start.11
  23.1 132.1 %all-reduce.3.cloned.1.call-start = ((), (), s32[]{:S(2)}) async-start(), calls=%async_computation.6 | async-start | bytes 4194304 | tf_op jit(solution)/shard_map/psum | solution.py:152
  85.6 4.0 %copy-start.3 = (bf16[4,512,1024]{2,1,0:T(8,128)(2,1)S(1)}, bf16[4,512,1024]{2,1,0:T(8,128)(2,1)}, u32[]{:S(2)}) copy-start(bf16[4,512,1024]{2,1,0:T(8,128)(2,1)} %param.41) | copy-start | bytes 12582916
  91.4 97.0 %reduce-scatter.5.cloned.1.call-start = ((), (), s32[]{:S(2)}) async-start(), calls=%async_computation.5 | async-start | bytes 589824 | tf_op jit(solution)/shard_map/reduce_scatter | solution.py:173
  158.8 5.0 %copy-start.2 = (f32[64,16,64]{2,0,1:T(8,128)S(1)}, f32[64,16,64]{2,0,1:T(8,128)}, u32[]{:S(2)}) copy-start(f32[64,16,64]{2,0,1:T(8,128)} %copy-done.1) | copy-start | bytes 786436
  159.7 28.7 %all-to-all-start.1 = ((bf16[4,128,512]{2,1,0:T(8,128)(2,1)}), bf16[4,128,512]{2,1,0:T(8,128)(2,1)}, u32[]{:S(2)}, u32[]{:S(2)}) async-start(bf16[4,128,512]{2,1,0:T(8,128)(2,1)} %bitcast.100), calls=%async_computation.3 | async-start | bytes 1048576 | tf_op jit(solution)/shard_map/all_to_all | solution.py:158
  163.9 4.2 %copy-start.12 = (f32[64,4]{0,1:T(4,128)S(1)}, f32[64,4]{0,1:T(4,128)}, u32[]{:S(2)}) copy-start(f32[64,4]{0,1:T(4,128)} %param.45) | copy-start | bytes 3076
Sparse Core Ops, SparseCore 0:
  23.2 35.2 reduce-scatter.2
  91.5 63.6 all-reduce.2
  157.4 30.9 reduce-scatter.4
where the time goes:
time: 198 us; the launch traced here: 197 us
  waiting for transfers between devices  96 us (48%)
  blocking collectives  42.1 us (21%)
  matrix products  24.4 us (12%)
  between operations  14 us (7%)
  local copies, waits for them, and re-layouts  12 us (6%)
  starting transfers between devices  4.25 us (2%)
  other arithmetic  4.21 us (2%)
    psum x1, waiting for transfers between devices, local(): lax.psum(up_part.astype(jnp.bfloat16), 'tp').astype(jnp.float32)  42.7 us
    reduce_scatter x1, waiting for transfers between devices, local(): lax.psum_scatter(mixer_terms, 'tp', scatter_dimension=1, tiled=True)  33.1 us
    reduce_scatter x1, waiting for transfers between devices, local(): lax.psum_scatter(shared_terms.astype(jnp.bfloat16), 'tp', scatter_dimensi...  20.2 us
    all_gather x1, blocking collectives, local(): ffn_rows = lax.all_gather(rows_own, 'tp', axis=1, tiled=True)  16.5 us
    psum x1, blocking collectives, local(): lax.psum(jnp.sum(resid_f * resid_f, axis=1, keepdims=True), 'tp')  13.9 us
    all_to_all x1, blocking collectives, local(): lax.all_to_all(outgoing, 'ep', split_axis=0, concat_axis=0, tiled=True)  11.7 us
    all_to_all x1, starting transfers between devices, local(): lax.all_to_all(expert_terms.reshape(ep_count, expert_dev * capacity, slic...  4.13 us
    dot_general x1, matrix products, local(): jnp.einsum('secd,edf->secf', arrived, expert_up, preferred_element_type=j...  4.04 us
  transfers between devices with their start and end apart: 4, of which 3 were waited for; matrix products, arithmetic and copies ran while one was open for 8% of the time, Pallas kernels for 0%

commit v1 on v0

--- a/solution.py
+++ b/solution.py
@@ -149,7 +149,7 @@
     up_part = jnp.einsum("secd,edf->secf", arrived, expert_up, preferred_element_type=jnp.float32)
     gate_full, up_full = (
         lax.psum(gate_part.astype(jnp.bfloat16), "tp").astype(jnp.float32),
-        lax.psum(up_part.astype(jnp.bfloat16), "tp").astype(jnp.float32),
+        jnp.sum(lax.all_gather(up_part.astype(jnp.bfloat16), "tp"), axis=0).astype(jnp.float32),
     )
     inner_rows = (jax.nn.silu(gate_full) * up_full).astype(jnp.bfloat16)
     expert_terms = jnp.einsum(

time: 198 us -> 272 us (1.37)
  waiting for transfers between devices: 96 us -> 160 us
  other arithmetic: 4.21 us -> 11 us
    all_gather x0 -> x1, waiting for transfers between devices: none -> 53.8 us  [local(): lax.all_gather(up_part.astype(jnp.bfloat16), 'tp')]
    psum x1, waiting for transfers between devices: 42.7 us -> 53.7 us  [local(): lax.psum(gate_part.astype(jnp.bfloat16), 'tp').astype(jnp.float32)]
    reduce_sum x0 -> x1, other arithmetic: none -> 6.76 us  [local(): jnp.sum(lax.all_gather(up_part.astype(jnp.bfloat16), 'tp'), axis=0)]
  transfers between devices with their start and end apart: 4 -> 5, of which waited for: 3 -> 4; matrix products, arithmetic and copies ran while one was open for 8% -> 10% of each run, Pallas kernels for 0% -> 0%
where the time goes in v1:
time: 272 us
  waiting for transfers between devices  160 us (59%)
  blocking collectives  42.8 us (16%)
  matrix products  26.6 us (10%)
  between operations  14 us (5%)
  local copies, waits for them, and re-layouts  13 us (5%)
  other arithmetic  11 us (4%)
  starting transfers between devices  4.29 us (2%)
    all_gather x1, waiting for transfers between devices, local(): lax.all_gather(up_part.astype(jnp.bfloat16), 'tp')  53.8 us
    psum x1, waiting for transfers between devices, local(): lax.psum(gate_part.astype(jnp.bfloat16), 'tp').astype(jnp.float32)  53.7 us
    reduce_scatter x1, waiting for transfers between devices, local(): lax.psum_scatter(mixer_terms, 'tp', scatter_dimension=1, tiled=True)  33.1 us
    reduce_scatter x1, waiting for transfers between devices, local(): lax.psum_scatter(shared_terms.astype(jnp.bfloat16), 'tp', scatter_dimensi...  19.4 us
    all_gather x1, blocking collectives, local(): ffn_rows = lax.all_gather(rows_own, 'tp', axis=1, tiled=True)  17.2 us
    psum x1, blocking collectives, local(): lax.psum(jnp.sum(resid_f * resid_f, axis=1, keepdims=True), 'tp')  13.8 us
    all_to_all x1, blocking collectives, local(): lax.all_to_all(outgoing, 'ep', split_axis=0, concat_axis=0, tiled=True)  11.7 us
    reduce_sum x1, other arithmetic, local(): jnp.sum(lax.all_gather(up_part.astype(jnp.bfloat16), 'tp'), axis=0)  6.76 us
  transfers between devices with their start and end apart: 5, of which 4 were waited for; matrix products, arithmetic and copies ran while one was open for 10% of the time, Pallas kernels for 0%

profile of v1, /device:TPU:0, one launch (start us, length us, event | category | flops | bytes accessed | tf_op | source)
XLA Modules:
  0.0 271.7 jit_solution(17364498877475678323)
XLA Ops:
  7.3 0.8 exp.27
  8.1 1.2 fusion.34
  9.4 0.8 reshape.245
  10.1 0.8 mul.328
  11.7 2.3 convolution_convert_fusion.2
  15.3 1.9 reshape.247
  17.7 1.8 bitcast_add_fusion
  19.5 0.9 fusion.55
  20.5 1.0 fusion.50
  21.5 1.5 fusion.75
  24.5 0.8 dynamic_slice.7
  25.4 33.1 %reduce-scatter.3.cloned.1.call-done = f32[64,512]{1,0:T(8,128)} async-done(((f32[64,4096]{1,0:T(8,128)}), f32[64,512]{1,0:T(8,128)}) %reduce-scatter.3.cloned.1.call-update) | async-done | bytes 131088 | tf_op jit(solution)/shard_map/reduce_scatter | solution.py:116
  58.5 1.0 fusion.51
  59.5 13.8 %psum.14 = f32[64,1]{0,1:T(1,128)S(1)} all-reduce(f32[64,1]{0,1:T(1,128)S(1)} %bitcast.107), channel_id=1, replica_groups=mesh['ep'=4,'tp'=8] {'tp'}, use_global_device_ids=true, to_apply=%region_3.0 | all-reduce | flops 64 | bytes 512 | tf_op jit(solution)/shard_map/psum | solution.py:120
  73.8 11.7 %all_to_all.10 = bf16[4,128,512]{2,1,0:T(8,128)(2,1)S(1)} all-to-all(bf16[4,128,512]{2,1,0:T(8,128)(2,1)S(1)} %bitcast.101), channel_id=1, replica_groups=mesh['ep'=4,'tp'=8] {'ep'}, dimensions={0} | all-to-all | bytes 1048576 | tf_op jit(solution)/shard_map/all_to_all | solution.py:144
  85.5 0.8 copy-done.3
  86.3 3.9 %fusion.17 = bf16[4,4,32,1024]{3,2,0,1:T(8,128)(2,1)} fusion(bf16[4,512,1024]{2,1,0:T(8,128)(2,1)} %param.42, bf16[4,4,32,512]{3,2,1,0:T(8,128)(2,1)S(1)} %bitcast.99), kind=kOutput, calls=%fused_computation.16 | convolution fusion | flops 537395200 | bytes 5767168 | tf_op jit(solution)/shard_map/secd,edf->secf/dot_general | solution.py:149
  90.2 17.2 %all_gather.9 = bf16[64,4096]{1,0:T(8,128)(2,1)S(1)} all-gather(bf16[64,512]{1,0:T(8,128)(2,1)S(1)} %fusion.53), channel_id=1, replica_groups=mesh['ep'=4,'tp'=8] {'tp'}, dimensions={1}, use_global_device_ids=true | all-gather | bytes 589824 | tf_op jit(solution)/shard_map/all_gather | solution.py:124
  107.5 4.2 %fusion.20 = bf16[4,4,32,1024]{3,2,0,1:T(8,128)(2,1)} fusion(bf16[4,512,1024]{2,1,0:T(8,128)(2,1)} %param.41, bf16[4,4,32,512]{3,2,1,0:T(8,128)(2,1)} %bitcast.100), kind=kOutput, calls=%fused_computation.17 | convolution fusion | flops 537395200 | bytes 5767168 | tf_op jit(solution)/shard_map/secd,edf->secf/dot_general | solution.py:146
  111.8 1.5 fusion.76
  113.3 3.0 %convolution_convert_fusion = bf16[64,4096]{1,0:T(8,128)(2,1)} fusion(bf16[128,4096]{1,0:T(8,128)(2,1)} %param.40, bf16[64,4096]{1,0:T(8,128)(2,1)S(1)} %all_gather.9, bf16[4096,128]{1,0:T(8,128)(2,1)} %param.39, f32[64,128]{1,0:T(8,128)S(1)} %fusion.76), kind=kOutput, calls=%fused_computation | convolution fusion | flops 134529024 | bytes 3178496 | tf_op jit(solution)/shard_map/dot_general | solution.py:172
  116.3 53.8 %all-gather.3.cloned.1.call-done = bf16[32,4,32,1024]{3,2,0,1:T(8,128)(2,1)} async-done(((bf16[4,4,32,1024]{3,2,0,1:T(8,128)(2,1)}), bf16[32,4,32,1024]{3,2,0,1:T(8,128)(2,1)}) %all-gather.3.cloned.1.call-update) | async-done | bytes 8388624 | tf_op jit(solution)/shard_map/all_gather | solution.py:152
  170.1 6.8 %reduce_sum.75 = bf16[4,4,32,1024]{3,2,0,1:T(8,128)(2,1)} reduce(bf16[8,4,4,32,1024]{4,3,1,0,2:T(8,128)(2,1)} %bitcast.98, bf16[]{:T(256)} %constant.42.clone.1), dimensions={0}, to_apply=%region_12.13 | reduce | flops 3670016 | bytes 9437186 | tf_op jit(solution)/shard_map/reduce_sum | solution.py:152
  176.9 53.7 %all-reduce.2.cloned.1.call-done = bf16[4,4,32,1024]{3,2,0,1:T(8,128)(2,1)} async-done(((bf16[4,4,32,1024]{3,2,0,1:T(8,128)(2,1)}), bf16[4,4,32,1024]{3,2,0,1:T(8,128)(2,1)}) %all-reduce.2.cloned.1.call-update) | async-done | bytes 1048592 | tf_op jit(solution)/shard_map/psum | solution.py:151
  230.6 3.7 %fusion.26 = bf16[4,4,32,512]{3,2,0,1:T(8,128)(2,1)S(1)} fusion(bf16[4,1024,512]{2,1,0:T(8,128)(2,1)} %param.43, bf16[4,4,32,1024]{3,2,0,1:T(8,128)(2,1)} %reduce_sum.75, bf16[4,4,32,1024]{3,2,0,1:T(8,128)(2,1)} %all-reduce.2.cloned.1.call-done), kind=kOutput, calls=%fused_computation.22 | convolution fusion | flops 541327360 | bytes 6815744 | tf_op jit(solution)/shard_map/secf,efd->secd/dot_general | solution.py:155
  234.3 0.9 copy.92
  235.2 4.1 %all-to-all-start.1 = ((bf16[4,128,512]{2,1,0:T(8,128)(2,1)}), bf16[4,128,512]{2,1,0:T(8,128)(2,1)}, u32[]{:S(2)}, u32[]{:S(2)}) async-start(bf16[4,128,512]{2,1,0:T(8,128)(2,1)} %bitcast.102), calls=%async_computation.3 | async-start | bytes 1048576 | tf_op jit(solution)/shard_map/all_to_all | solution.py:158
  239.3 1.1 copy.94
  240.8 1.9 reshape.259
  242.7 0.9 reshape.258
  243.7 19.4 %reduce-scatter.5.cloned.1.call-done = bf16[64,512]{1,0:T(8,128)(2,1)} async-done(((bf16[64,4096]{1,0:T(8,128)(2,1)}), bf16[64,512]{1,0:T(8,128)(2,1)}) %reduce-scatter.5.cloned.1.call-update) | async-done | bytes 65552 | tf_op jit(solution)/shard_map/reduce_scatter | solution.py:173
  263.1 2.1 fusion.31
  (64 shorter events, 5.3 us)
Async XLA Ops:
  7.2 14.3 %copy-start = (bf16[256,4096]{1,0:T(8,128)(2,1)S(1)}, bf16[256,4096]{1,0:T(8,128)(2,1)}, u32[]{:S(2)}) copy-start(bf16[256,4096]{1,0:T(8,128)(2,1)} %param.37) | copy-start | bytes 6291460
  7.2 7.0 %copy-start.6 = (f32[16,1024]{1,0:T(8,128)S(1)}, f32[16,1024]{1,0:T(8,128)}, u32[]{:S(2)}) copy-start(f32[16,1024]{1,0:T(8,128)} %param.30) | copy-start | bytes 196612
  7.2 7.0 %copy-start.7 = (f32[16,1024]{1,0:T(8,128)S(1)}, f32[16,1024]{1,0:T(8,128)}, u32[]{:S(2)}) copy-start(f32[16,1024]{1,0:T(8,128)} %param.31) | copy-start | bytes 196612
  7.2 7.1 %copy-start.8 = (f32[16,1024]{1,0:T(8,128)S(1)}, f32[16,1024]{1,0:T(8,128)}, u32[]{:S(2)}) copy-start(f32[16,1024]{1,0:T(8,128)} %param.32) | copy-start | bytes 196612
  7.2 7.9 %copy-start.9 = (f32[16,1024]{1,0:T(8,128)S(1)}, f32[16,1024]{1,0:T(8,128)}, u32[]{:S(2)}) copy-start(f32[16,1024]{1,0:T(8,128)} %param.33) | copy-start | bytes 196612
  7.2 7.9 %copy-start.5 = (f32[64,1024]{1,0:T(8,128)S(1)}, f32[64,1024]{1,0:T(8,128)}, u32[]{:S(2)}) copy-start(f32[64,1024]{1,0:T(8,128)} %param.35) | copy-start | bytes 786436
  7.2 51.2 %reduce-scatter.3.cloned.1.call-start = ((), (), s32[]{:S(2)}) async-start(), calls=%async_computation.4 | async-start | bytes 1179648 | tf_op jit(solution)/shard_map/reduce_scatter | solution.py:116
  17.2 2.4 copy-start.4
  19.5 1.0 copy-start.1
  21.5 1.6 copy-start.10
  23.0 147.1 %all-gather.3.cloned.1.call-start = ((), (), s32[]{:S(2)}) async-start(), calls=%async_computation.7 | async-start | bytes 9437184 | tf_op jit(solution)/shard_map/all_gather | solution.py:152
  85.5 0.8 copy-start.3
  90.2 140.4 %all-reduce.2.cloned.1.call-start = ((), (), s32[]{:S(2)}) async-start(), calls=%async_computation.6 | async-start | bytes 2097152 | tf_op jit(solution)/shard_map/psum | solution.py:151
  111.7 151.4 %reduce-scatter.5.cloned.1.call-start = ((), (), s32[]{:S(2)}) async-start(), calls=%async_computation.5 | async-start | bytes 589824 | tf_op jit(solution)/shard_map/reduce_scatter | solution.py:173
  234.3 5.0 %copy-start.2 = (f32[64,16,64]{2,0,1:T(8,128)S(1)}, f32[64,16,64]{2,0,1:T(8,128)}, u32[]{:S(2)}) copy-start(f32[64,16,64]{2,0,1:T(8,128)} %copy-done.1) | copy-start | bytes 786436
  235.2 28.0 %all-to-all-start.1 = ((bf16[4,128,512]{2,1,0:T(8,128)(2,1)}), bf16[4,128,512]{2,1,0:T(8,128)(2,1)}, u32[]{:S(2)}, u32[]{:S(2)}) async-start(bf16[4,128,512]{2,1,0:T(8,128)(2,1)} %bitcast.102), calls=%async_computation.3 | async-start | bytes 1048576 | tf_op jit(solution)/shard_map/all_to_all | solution.py:158
  239.3 4.2 %copy-start.11 = (f32[64,4]{0,1:T(4,128)S(1)}, f32[64,4]{0,1:T(4,128)}, u32[]{:S(2)}) copy-start(f32[64,4]{0,1:T(4,128)} %param.45) | copy-start | bytes 3076
Sparse Core Ops, SparseCore 0:
  23.1 35.3 reduce-scatter.2
  90.3 79.7 all-gather.2
  172.5 58.1 all-reduce.1
  232.7 30.3 reduce-scatter.4
